TPU v7x, 32 devices: a whole 2x2x4 slice. The times are simulated.
32 devices in a mesh: sp: 16 (over z, y, core), tp: 2 (over x).
Axes of the slice: x: 2, y: 2, z: 4, core: 2. Of those that a mesh axis runs over, the one named last changes fastest.
Arguments:
- glu_value: bfloat16 [8192, 1024], P('sp', 'tp'), may hold values from -6 to 6
- glu_gate: bfloat16 [8192, 1024], P('sp', 'tp'), may hold values from -8 to 8
- conv_taps: float32 [31, 1024], P(None, 'tp'), may hold values from -1 to 1
- channel_norm_gain: float32 [1024], P('tp'), may hold values from 0.1 to 1.9
- channel_norm_bias: float32 [1024], P('tp'), may hold values from -3 to 3
- out_proj: bfloat16 [1024, 2048], P('tp'), may hold values from -0.1875 to 0.1875
- out_grad: bfloat16 [8192, 2048], P('sp'), may hold values from -6 to 6
Outputs:
- grad_value: bfloat16 [8192, 1024], P('sp', 'tp')
- grad_gate: bfloat16 [8192, 1024], P('sp', 'tp')
- grad_taps: float32 [31, 1024], P(None, 'tp')
- norm_gain_gradient: float32 [1024], P('tp')
- grad_bias: float32 [1024], P('tp')
- grad_proj: float32 [2048, 1024], P('sp', 'tp')
All inputs are finite; a program needn't handle non-finite values.
Results may differ from a plain program's by a relative error of at most 0.0049.
Values may be sent and summed in bfloat16 or wider, within the bound.
A program may use at most 64 MiB of HBM per device.

v0:
```python
import jax
import jax.numpy as jnp
from jax import lax
from jax.sharding import PartitionSpec as P

CONV_CHANNELS = 1024
TAPS = 31


def passed_along(shard, axis, by):
    size = lax.axis_size(axis)
    pairs = [(i, i + by) for i in range(size) if 0 <= i + by < size]
    return lax.ppermute(shard, axis, pairs)


def on_device(
    glu_value, glu_gate, conv_taps, channel_norm_gain, channel_norm_bias, out_proj, out_grad
):
    rows, width = glu_value.shape
    value = glu_value.astype(jnp.float32)
    sig_gate = jax.nn.sigmoid(glu_gate.astype(jnp.float32))
    gated = (value * sig_gate).astype(jnp.bfloat16)
    before = passed_along(gated[rows - (TAPS - 1) :], "sp", 1)
    padded = jnp.concatenate([before, gated], axis=0).astype(jnp.float32)
    conv_output = jnp.zeros((rows, width), jnp.float32)
    for k in range(TAPS):
        conv_output = conv_output + conv_taps[k][None, :] * padded[k : k + rows]
    total, squares = lax.psum(
        (jnp.sum(conv_output, axis=1), jnp.sum(conv_output * conv_output, axis=1)), "tp"
    )
    channel_mean = (total / CONV_CHANNELS)[:, None]
    var = (squares / CONV_CHANNELS)[:, None] - channel_mean * channel_mean
    inverse_deviation = lax.rsqrt(var + 1e-05)
    centered_standardized = (conv_output - channel_mean) * inverse_deviation
    normalized_rows = (
        centered_standardized * channel_norm_gain[None, :] + channel_norm_bias[None, :]
    )
    sig_norm = jax.nn.sigmoid(normalized_rows)
    act = (normalized_rows * sig_norm).astype(jnp.bfloat16)
    grad_act = lax.dot_general(
        out_grad, out_proj, (((1,), (1,)), ((), ())), preferred_element_type=jnp.float32
    )
    grad_proj = lax.psum_scatter(
        lax.dot_general(
            out_grad, act, (((0,), (0,)), ((), ())), preferred_element_type=jnp.float32
        ),
        "sp",
        scatter_dimension=0,
        tiled=True,
    )
    normalized_gradient = grad_act * sig_norm * (1.0 + normalized_rows * (1.0 - sig_norm))
    scaled_rows = normalized_gradient * channel_norm_gain[None, :]
    first_term, second_term = lax.psum(
        (jnp.sum(scaled_rows, axis=1), jnp.sum(scaled_rows * centered_standardized, axis=1)), "tp"
    )
    conv_output_gradient = inverse_deviation * (
        scaled_rows
        - (first_term / CONV_CHANNELS)[:, None]
        - centered_standardized * (second_term / CONV_CHANNELS)[:, None]
    )
    taps_local = jnp.stack(
        [jnp.sum(conv_output_gradient * padded[k : k + rows], axis=0) for k in range(TAPS)], axis=0
    )
    packed = jnp.concatenate(
        [
            taps_local,
            jnp.sum(normalized_gradient * centered_standardized, axis=0)[None, :],
            jnp.sum(normalized_gradient, axis=0)[None, :],
        ],
        axis=0,
    )
    share = lax.psum_scatter(packed, "sp", scatter_dimension=1, tiled=True)
    summed = lax.all_gather(share, "sp", axis=1, tiled=True)
    ahead = passed_along(conv_output_gradient[: TAPS - 1], "sp", -1)
    after = jnp.concatenate([conv_output_gradient, ahead], axis=0)
    grad_gated = jnp.zeros((rows, width), jnp.float32)
    for k in range(TAPS):
        grad_gated = grad_gated + conv_taps[k][None, :] * after[TAPS - 1 - k : TAPS - 1 - k + rows]
    grad_value = (grad_gated * sig_gate).astype(jnp.bfloat16)
    grad_gate = (grad_gated * value * sig_gate * (1.0 - sig_gate)).astype(jnp.bfloat16)
    return (grad_value, grad_gate, summed[:TAPS], summed[TAPS], summed[TAPS + 1], grad_proj)


def solution(mesh):
    return jax.shard_map(
        on_device,
        mesh=mesh,
        in_specs=(
            P("sp", "tp"),
            P("sp", "tp"),
            P(None, "tp"),
            P("tp"),
            P("tp"),
            P("tp", None),
            P("sp", None),
        ),
        out_specs=(P("sp", "tp"), P("sp", "tp"), P(None, "tp"), P("tp"), P("tp"), P("sp", "tp")),
        check_vma=False,
    )
```

profile of v0, /device:TPU:0, one launch (start us, length us, event | category | flops | bytes accessed | tf_op | source)
XLA Modules:
  0.0 184.4 jit_solution(906869488730801096)
XLA Ops:
  7.2 0.0 copy-start
  7.2 0.0 reduce-scatter.7.cloned.1.call-start
  7.2 1.6 fusion.1
  8.9 2.4 %collective-permute-start = (bf16[30,512]{1,0:T(8,128)(2,1)S(1)}, bf16[30,512]{1,0:T(8,128)(2,1)S(1)}, u32[]{:S(2)}, u32[]{:S(2)}) collective-permute-start(bf16[30,512]{1,0:T(8,128)(2,1)S(1)} %slice.450), channel_id=1, source_target_pairs={{0,2},{2,4},{4,6},{6,8},{8,10},{10,12},{12,14},{14,16},{16,18},{18... | collective-permute-start | bytes 92168 | tf_op jit(solution)/shard_map/ppermute | solution.py:13
  11.3 1.1 fusion.101
  12.4 1.0 fusion.102
  13.5 0.0 collective-permute-done
  13.5 0.2 maximum_convert_fusion
  13.6 0.0 copy-start.4
  13.6 0.0 copy-start.5
  13.7 5.7 %multiply_reduce_fusion.33 = (f32[512]{0:T(512)S(1)}, f32[512]{0:T(512)S(1)}, f32[512,512]{1,0:T(8,128)}) fusion(f32[542,512]{1,0:T(8,128)S(1)} %maximum_convert_fusion, f32[512]{0:T(512)S(1)} %bitcast.132, f32[512]{0:T(512)S(1)} %bitcast.134, f32[512]{0:T(512)S(1)} %bitcast.76, f32[512]{0:T(512)S(1)} %bitcast.78, f32[512]{0:T(512)S(1)} %bitcast.80, ...), kind=kLoop, calls=%fused_computation.184 | loop fusion | flops 16776192 | bytes 33622016 | tf_op jit(solution)/shard_map/reduce_sum | solution.py:29
  19.4 5.2 %all-reduce.1 = (f32[512]{0:T(512)S(1)}, f32[512]{0:T(512)S(1)}) all-reduce(f32[512]{0:T(512)S(1)} %get-tuple-element.60, f32[512]{0:T(512)S(1)} %get-tuple-element.59), channel_id=1, replica_groups=mesh['sp'=16,'tp'=2] {'tp'}, use_global_device_ids=true, to_apply=%region_3.0 | all-reduce | flops 1024 | bytes 8192 | tf_op jit(solution)/shard_map/psum | solution.py:28
  24.6 0.0 copy-done
  24.6 0.0 copy-done.4
  24.6 0.0 copy-done.5
  24.6 4.6 %multiply_reduce_fusion = (f32[512]{0:T(512)S(1)}, f32[512]{0:T(512)S(1)}, f32[512]{0:T(512)S(1)}, f32[512]{0:T(512)S(1)}, f32[512,512]{1,0:T(8,128)}) fusion(f32[512,512]{1,0:T(8,128)} %get-tuple-element.70, f32[512]{0:T(512)S(1)} %get-tuple-element.103, f32[512]{0:T(512)S(1)} %get-tuple-element.102, f32[512]{0:T(512)S(1)} %copy-done.4, ...), kind=kOutput, calls=%fused_computation.146 | convolution fusion | flops 1078720512 | bytes 6307840 | tf_op jit(solution)/shard_map/dot_general | solution.py:40
  29.2 4.9 %all-reduce = (f32[512]{0:T(512)S(1)}, f32[512]{0:T(512)S(1)}) all-reduce(f32[512]{0:T(512)S(1)} %get-tuple-element.56, f32[512]{0:T(512)S(1)} %get-tuple-element.57), channel_id=1, replica_groups=mesh['sp'=16,'tp'=2] {'tp'}, use_global_device_ids=true, to_apply=%region_7.0 | all-reduce | flops 1024 | bytes 8192 | tf_op jit(solution)/shard_map/psum | solution.py:53
  34.1 4.2 %multiply_reduce_fusion.1 = (f32[512]{0:T(512)S(1)}, f32[512]{0:T(512)S(1)}, f32[512]{0:T(512)S(1)}, f32[512]{0:T(512)S(1)}, f32[512]{0:T(512)S(1)}, /*index=5*/...) fusion(f32[542,512]{1,0:T(8,128)S(1)} %maximum_convert_fusion, ...), kind=kLoop, calls=%fused_computation.147 | loop fusion | flops 11262976 | bytes 22067200 | tf_op jit(solution)/shard_map/reduce_sum | solution.py:62
  38.3 0.0 copy-start.1
  38.3 1.7 multiply_reduce_fusion.19
  40.0 0.0 copy-done.1
  40.0 0.2 concatenate.11
  40.2 0.8 copy.20
  41.0 0.0 reduce-scatter.7.cloned.1.call-update
  41.1 0.0 reduce-scatter.5.cloned.1.call-start
  41.1 4.6 %convolution_bitcast_fusion = f32[2048,512]{0,1:T(8,128)} fusion(bf16[512,2048]{1,0:T(8,128)(2,1)S(1)} %copy-done, f32[512,512]{1,0:T(8,128)} %get-tuple-element.70, f32[512]{0:T(512)S(1)} %copy-done.5, f32[512]{0:T(512)S(1)} %copy-done.4, f32[512]{0:T(512)S(1)} %get-tuple-element.103, f32[512]{0:T(512)S(1)} %get-tuple-element.102), kind=kOutput, calls=%fused_computation.29 | convolution fusion | flops 1076101120 | bytes 7348224 | tf_op jit(solution)/shard_map/dot_general | solution.py:44
  45.7 0.0 copy-start.2
  45.7 0.0 reduce-scatter.5.cloned.1.call-update
  45.8 1.2 copy-done.2
  47.0 0.0 copy-start.3
  47.0 1.4 collective-permute-start.1
  48.4 1.8 %collective-permute-done.1 = f32[30,512]{1,0:T(8,128)S(1)} collective-permute-done((f32[30,512]{1,0:T(8,128)S(1)}, f32[30,512]{1,0:T(8,128)S(1)}, u32[]{:S(2)}, u32[]{:S(2)}) %collective-permute-start.1) | collective-permute-done | bytes 61472 | tf_op jit(solution)/shard_map/ppermute | solution.py:13
  50.2 7.0 %fusion.4 = (bf16[512,512]{1,0:T(8,128)(2,1)}, f32[512,512]{1,0:T(8,128)S(1)}) fusion(bf16[512,512]{1,0:T(8,128)(2,1)} %param.7, bf16[512,512]{1,0:T(8,128)(2,1)} %param.8, f32[512,512]{1,0:T(8,128)S(1)} %copy-done.2, f32[512]{0:T(512)S(1)} %bitcast.133, f32[30,512]{1,0:T(8,128)S(1)} %collective-permute-done.1, f32[512]{0:T(512)S(1)} %bitcast.135, ...), kind=kLoop, calls=%fused_computation.37 | loop fusion | flops 26476544 | bytes 3794944 | tf_op jit(solution)/shard_map/convert_element_type | solution.py:80
  57.2 0.0 copy-done.3
  57.2 1.1 multiply_convert_fusion.1
  58.3 41.8 %reduce-scatter.7.cloned.1.call-done = f32[32,33]{1,0:T(8,128)} async-done(((f32[512,33]{1,0:T(8,128)}), f32[32,33]{1,0:T(8,128)}) %reduce-scatter.7.cloned.1.call-update) | async-done | bytes 4240
  100.1 20.3 %all_gather.3 = f32[33,512]{0,1:T(8,128)S(1)} all-gather(f32[33,32]{0,1:T(8,128)} %bitcast.136), channel_id=1, replica_groups=mesh['sp'=16,'tp'=2] {'sp'}, dimensions={1}, use_global_device_ids=true | all-gather | bytes 71808 | tf_op jit(solution)/shard_map/all_gather | solution.py:73
  120.4 0.7 copy.18
  121.2 1.0 slice_reduce_fusion
  122.1 53.6 %reduce-scatter.5.cloned.1.call-done = f32[128,512]{0,1:T(8,128)} async-done(((f32[2048,512]{0,1:T(8,128)}), f32[128,512]{0,1:T(8,128)}) %reduce-scatter.5.cloned.1.call-update) | async-done | bytes 262160 | tf_op jit(solution)/shard_map/reduce_scatter | solution.py:43
  175.8 1.8 copy.19
  (4 shorter events, 0.0 us)
Async XLA Ops:
  7.2 17.4 %copy-start = (bf16[512,2048]{1,0:T(8,128)(2,1)S(1)}, bf16[512,2048]{1,0:T(8,128)(2,1)}, u32[]{:S(2)}) copy-start(bf16[512,2048]{1,0:T(8,128)(2,1)} %param.13) | copy-start | bytes 6291460
  7.2 92.9 %reduce-scatter.7.cloned.1.call-start = ((), (), s32[]{:S(2)}) async-start(), calls=%async_computation.3 | async-start | bytes 278528
  8.9 4.6 %collective-permute-start = (bf16[30,512]{1,0:T(8,128)(2,1)S(1)}, bf16[30,512]{1,0:T(8,128)(2,1)S(1)}, u32[]{:S(2)}, u32[]{:S(2)}) collective-permute-start(bf16[30,512]{1,0:T(8,128)(2,1)S(1)} %slice.450), channel_id=1, source_target_pairs={{0,2},{2,4},{4,6},{6,8},{8,10},{10,12},{12,14},{14,16},{16,18},{18... | collective-permute-start | bytes 92168 | tf_op jit(solution)/shard_map/ppermute | solution.py:13
  13.6 11.0 %copy-start.4 = (f32[512]{0:T(512)S(1)}, f32[512]{0:T(512)}, u32[]{:S(2)}) copy-start(f32[512]{0:T(512)} %param.10) | copy-start | bytes 6148
  13.6 11.0 %copy-start.5 = (f32[512]{0:T(512)S(1)}, f32[512]{0:T(512)}, u32[]{:S(2)}) copy-start(f32[512]{0:T(512)} %param.11) | copy-start | bytes 6148
  38.3 1.7 copy-start.1
  41.1 134.7 %reduce-scatter.5.cloned.1.call-start = ((), (), s32[]{:S(2)}) async-start(), calls=%async_computation.2 | async-start | bytes 4456448 | tf_op jit(solution)/shard_map/reduce_scatter | solution.py:43
  45.7 1.2 copy-start.2
  47.0 10.3 %copy-start.3 = (bf16[512,512]{1,0:T(8,128)(2,1)S(1)}, bf16[512,512]{1,0:T(8,128)(2,1)}, u32[]{:S(2)}) copy-start(bf16[512,512]{1,0:T(8,128)(2,1)} %param.8) | copy-start | bytes 1572868
  47.0 3.3 %collective-permute-start.1 = (f32[30,512]{1,0:T(8,128)S(1)}, f32[30,512]{1,0:T(8,128)S(1)}, u32[]{:S(2)}, u32[]{:S(2)}) collective-permute-start(f32[30,512]{1,0:T(8,128)S(1)} %slice.482), channel_id=1, source_target_pairs={{2,0},{4,2},{6,4},{8,6},{10,8},{12,10},{14,12},{16,14},{18,16},{20... | collective-permute-start | bytes 184328 | tf_op jit(solution)/shard_map/ppermute | solution.py:13
Sparse Core Ops, SparseCore 0:
  41.2 58.8 reduce-scatter.6
  103.9 71.7 reduce-scatter.4
where the time goes:
time: 185 us; the launch traced here: 184 us
  waiting for transfers between devices  97.3 us (53%)
  blocking collectives  30.4 us (16%)
  other arithmetic  21.5 us (12%)
  between operations  14.2 us (8%)
  matrix products  9.17 us (5%)
  local copies, waits for them, and re-layouts  7.9 us (4%)
  starting transfers between devices  3.9 us (2%)
    reduce_scatter x1, waiting for transfers between devices, on_device(): lax.psum_scatter(lax.dot_general(out_grad, act, (((0,), (0,)), ((), ())),...  53.6 us
    unnamed x3, waiting for transfers between devices  41.8 us
    all_gather x1, blocking collectives, on_device(): summed = lax.all_gather(share, 'sp', axis=1, tiled=True)  20.3 us
    convert_element_type x1, other arithmetic, on_device(): (grad_gated * value * sig_gate * (1.0 - sig_gate)).astype(jnp.bfloat16)  6.99 us
    reduce_sum x2, other arithmetic, on_device(): jnp.sum(conv_output_gradient * padded[k:k + rows], axis=0)  5.89 us
    reduce_sum x1, other arithmetic, on_device(): jnp.sum(conv_output * conv_output, axis=1)  5.75 us
    psum x1, blocking collectives, on_device(): lax.psum((jnp.sum(conv_output, axis=1), jnp.sum(conv_output * conv_output...  5.19 us
    psum x1, blocking collectives, on_device(): lax.psum((jnp.sum(scaled_rows, axis=1), jnp.sum(scaled_rows * centered_st...  4.91 us
  transfers between devices with their start and end apart: 4, of which 3 were waited for; matrix products, arithmetic and copies ran while one was open for 9% of the time, Pallas kernels for 0%

commit v1 on v0

--- a/solution.py
+++ b/solution.py
@@ -70,7 +70,7 @@
         axis=0,
     )
     share = lax.psum_scatter(packed, "sp", scatter_dimension=1, tiled=True)
-    summed = lax.all_gather(share, "sp", axis=1, tiled=True)
+    summed = jnp.concatenate(lax.all_gather(share, "sp"), axis=1)
     ahead = passed_along(conv_output_gradient[: TAPS - 1], "sp", -1)
     after = jnp.concatenate([conv_output_gradient, ahead], axis=0)
     grad_gated = jnp.zeros((rows, width), jnp.float32)

time: 185 us -> 185 us (level)
  no operation moved by 1% of the time
where the time goes in v1:
time: 185 us; the launch traced here: 184 us
  waiting for transfers between devices  96.5 us (52%)
  blocking collectives  30.4 us (16%)
  other arithmetic  21.5 us (12%)
  between operations  14.2 us (8%)
  matrix products  9.17 us (5%)
  local copies, waits for them, and re-layouts  8.63 us (5%)
  starting transfers between devices  3.9 us (2%)
    reduce_scatter x1, waiting for transfers between devices, on_device(): lax.psum_scatter(lax.dot_general(out_grad, act, (((0,), (0,)), ((), ())),...  52.9 us
    unnamed x3, waiting for transfers between devices  41.8 us
    all_gather x1, blocking collectives, on_device(): summed = jnp.concatenate(lax.all_gather(share, 'sp'), axis=1)  20.3 us
    convert_element_type x1, other arithmetic, on_device(): (grad_gated * value * sig_gate * (1.0 - sig_gate)).astype(jnp.bfloat16)  6.99 us
    reduce_sum x2, other arithmetic, on_device(): jnp.sum(conv_output_gradient * padded[k:k + rows], axis=0)  5.89 us
    reduce_sum x1, other arithmetic, on_device(): jnp.sum(conv_output * conv_output, axis=1)  5.75 us
    psum x1, blocking collectives, on_device(): lax.psum((jnp.sum(conv_output, axis=1), jnp.sum(conv_output * conv_output...  5.19 us
    psum x1, blocking collectives, on_device(): lax.psum((jnp.sum(scaled_rows, axis=1), jnp.sum(scaled_rows * centered_st...  4.92 us
  transfers between devices with their start and end apart: 4, of which 3 were waited for; matrix products, arithmetic and copies ran while one was open for 9% of the time, Pallas kernels for 0%

profile of v1, /device:TPU:0, one launch (start us, length us, event | category | flops | bytes accessed | tf_op | source)
XLA Modules:
  0.0 184.4 jit_solution(194042830766719834)
XLA Ops:
  7.2 0.0 copy-start
  7.2 0.0 reduce-scatter.7.cloned.1.call-start
  7.2 1.6 fusion.1
  8.9 2.4 %collective-permute-start = (bf16[30,512]{1,0:T(8,128)(2,1)S(1)}, bf16[30,512]{1,0:T(8,128)(2,1)S(1)}, u32[]{:S(2)}, u32[]{:S(2)}) collective-permute-start(bf16[30,512]{1,0:T(8,128)(2,1)S(1)} %slice.456), channel_id=1, source_target_pairs={{0,2},{2,4},{4,6},{6,8},{8,10},{10,12},{12,14},{14,16},{16,18},{18... | collective-permute-start | bytes 92168 | tf_op jit(solution)/shard_map/ppermute | solution.py:13
  11.3 1.1 fusion.101
  12.4 1.0 fusion.102
  13.5 0.0 collective-permute-done
  13.5 0.2 maximum_convert_fusion
  13.6 0.0 copy-start.4
  13.6 0.0 copy-start.5
  13.7 5.7 %multiply_reduce_fusion.33 = (f32[512]{0:T(512)S(1)}, f32[512]{0:T(512)S(1)}, f32[512,512]{1,0:T(8,128)}) fusion(f32[542,512]{1,0:T(8,128)S(1)} %maximum_convert_fusion, f32[512]{0:T(512)S(1)} %bitcast.137, f32[512]{0:T(512)S(1)} %bitcast.139, f32[512]{0:T(512)S(1)} %bitcast.81, f32[512]{0:T(512)S(1)} %bitcast.83, f32[512]{0:T(512)S(1)} %bitcast.85, ...), kind=kLoop, calls=%fused_computation.184 | loop fusion | flops 16776192 | bytes 33622016 | tf_op jit(solution)/shard_map/reduce_sum | solution.py:29
  19.4 5.2 %all-reduce.1 = (f32[512]{0:T(512)S(1)}, f32[512]{0:T(512)S(1)}) all-reduce(f32[512]{0:T(512)S(1)} %get-tuple-element.66, f32[512]{0:T(512)S(1)} %get-tuple-element.65), channel_id=1, replica_groups=mesh['sp'=16,'tp'=2] {'tp'}, use_global_device_ids=true, to_apply=%region_3.0 | all-reduce | flops 1024 | bytes 8192 | tf_op jit(solution)/shard_map/psum | solution.py:28
  24.6 0.0 copy-done
  24.6 0.0 copy-done.4
  24.6 0.0 copy-done.5
  24.6 4.6 %multiply_reduce_fusion = (f32[512]{0:T(512)S(1)}, f32[512]{0:T(512)S(1)}, f32[512]{0:T(512)S(1)}, f32[512]{0:T(512)S(1)}, f32[512,512]{1,0:T(8,128)}) fusion(f32[512,512]{1,0:T(8,128)} %get-tuple-element.76, f32[512]{0:T(512)S(1)} %get-tuple-element.109, f32[512]{0:T(512)S(1)} %get-tuple-element.108, f32[512]{0:T(512)S(1)} %copy-done.4, ...), kind=kOutput, calls=%fused_computation.146 | convolution fusion | flops 1078720512 | bytes 6307840 | tf_op jit(solution)/shard_map/dot_general | solution.py:40
  29.2 4.9 %all-reduce = (f32[512]{0:T(512)S(1)}, f32[512]{0:T(512)S(1)}) all-reduce(f32[512]{0:T(512)S(1)} %get-tuple-element.62, f32[512]{0:T(512)S(1)} %get-tuple-element.63), channel_id=1, replica_groups=mesh['sp'=16,'tp'=2] {'tp'}, use_global_device_ids=true, to_apply=%region_7.0 | all-reduce | flops 1024 | bytes 8192 | tf_op jit(solution)/shard_map/psum | solution.py:53
  34.1 4.2 %multiply_reduce_fusion.1 = (f32[512]{0:T(512)S(1)}, f32[512]{0:T(512)S(1)}, f32[512]{0:T(512)S(1)}, f32[512]{0:T(512)S(1)}, f32[512]{0:T(512)S(1)}, /*index=5*/...) fusion(f32[542,512]{1,0:T(8,128)S(1)} %maximum_convert_fusion, ...), kind=kLoop, calls=%fused_computation.147 | loop fusion | flops 11262976 | bytes 22067200 | tf_op jit(solution)/shard_map/reduce_sum | solution.py:62
  38.3 0.0 copy-start.1
  38.3 1.7 multiply_reduce_fusion.19
  40.0 0.0 copy-done.1
  40.0 0.2 concatenate.11
  40.2 0.8 copy.22
  41.0 0.0 reduce-scatter.7.cloned.1.call-update
  41.1 0.0 reduce-scatter.5.cloned.1.call-start
  41.1 4.6 %convolution_bitcast_fusion = f32[2048,512]{0,1:T(8,128)} fusion(bf16[512,2048]{1,0:T(8,128)(2,1)S(1)} %copy-done, f32[512,512]{1,0:T(8,128)} %get-tuple-element.76, f32[512]{0:T(512)S(1)} %copy-done.5, f32[512]{0:T(512)S(1)} %copy-done.4, f32[512]{0:T(512)S(1)} %get-tuple-element.109, f32[512]{0:T(512)S(1)} %get-tuple-element.108), kind=kOutput, calls=%fused_computation.29 | convolution fusion | flops 1076101120 | bytes 7348224 | tf_op jit(solution)/shard_map/dot_general | solution.py:44
  45.7 0.0 copy-start.2
  45.7 0.0 reduce-scatter.5.cloned.1.call-update
  45.8 1.2 copy-done.2
  47.0 0.0 copy-start.3
  47.0 1.4 collective-permute-start.1
  48.4 1.8 %collective-permute-done.1 = f32[30,512]{1,0:T(8,128)S(1)} collective-permute-done((f32[30,512]{1,0:T(8,128)S(1)}, f32[30,512]{1,0:T(8,128)S(1)}, u32[]{:S(2)}, u32[]{:S(2)}) %collective-permute-start.1) | collective-permute-done | bytes 61472 | tf_op jit(solution)/shard_map/ppermute | solution.py:13
  50.2 7.0 %fusion.4 = (bf16[512,512]{1,0:T(8,128)(2,1)}, f32[512,512]{1,0:T(8,128)S(1)}) fusion(bf16[512,512]{1,0:T(8,128)(2,1)} %param.7, bf16[512,512]{1,0:T(8,128)(2,1)} %param.8, f32[512,512]{1,0:T(8,128)S(1)} %copy-done.2, f32[512]{0:T(512)S(1)} %bitcast.138, f32[30,512]{1,0:T(8,128)S(1)} %collective-permute-done.1, f32[512]{0:T(512)S(1)} %bitcast.140, ...), kind=kLoop, calls=%fused_computation.37 | loop fusion | flops 26476544 | bytes 3794944 | tf_op jit(solution)/shard_map/convert_element_type | solution.py:80
  57.2 0.0 copy-done.3
  57.2 1.1 multiply_convert_fusion.1
  58.3 41.8 %reduce-scatter.7.cloned.1.call-done = f32[32,33]{1,0:T(8,128)} async-done(((f32[512,33]{1,0:T(8,128)}), f32[32,33]{1,0:T(8,128)}) %reduce-scatter.7.cloned.1.call-update) | async-done | bytes 4240
  100.1 20.3 %all-gather.1 = f32[16,33,32]{1,2,0:T(8,128)S(1)} all-gather(f32[1,33,32]{1,2,0:T(8,128)} %bitcast.141), channel_id=2, replica_groups=mesh['sp'=16,'tp'=2] {'sp'}, dimensions={0}, use_global_device_ids=true | all-gather | bytes 71808 | tf_op jit(solution)/shard_map/all_gather | solution.py:73
  120.4 0.4 slice_reduce_fusion
  120.8 0.7 squeeze.7
  121.5 0.7 squeeze.6
  122.1 0.7 copy.20
  122.9 52.9 %reduce-scatter.5.cloned.1.call-done = f32[128,512]{0,1:T(8,128)} async-done(((f32[2048,512]{0,1:T(8,128)}), f32[128,512]{0,1:T(8,128)}) %reduce-scatter.5.cloned.1.call-update) | async-done | bytes 262160 | tf_op jit(solution)/shard_map/reduce_scatter | solution.py:43
  175.8 1.8 copy.21
  (4 shorter events, 0.0 us)
Async XLA Ops:
  7.2 17.4 %copy-start = (bf16[512,2048]{1,0:T(8,128)(2,1)S(1)}, bf16[512,2048]{1,0:T(8,128)(2,1)}, u32[]{:S(2)}) copy-start(bf16[512,2048]{1,0:T(8,128)(2,1)} %param.13) | copy-start | bytes 6291460
  7.2 92.9 %reduce-scatter.7.cloned.1.call-start = ((), (), s32[]{:S(2)}) async-start(), calls=%async_computation.3 | async-start | bytes 278528
  8.9 4.6 %collective-permute-start = (bf16[30,512]{1,0:T(8,128)(2,1)S(1)}, bf16[30,512]{1,0:T(8,128)(2,1)S(1)}, u32[]{:S(2)}, u32[]{:S(2)}) collective-permute-start(bf16[30,512]{1,0:T(8,128)(2,1)S(1)} %slice.456), channel_id=1, source_target_pairs={{0,2},{2,4},{4,6},{6,8},{8,10},{10,12},{12,14},{14,16},{16,18},{18... | collective-permute-start | bytes 92168 | tf_op jit(solution)/shard_map/ppermute | solution.py:13
  13.6 11.0 %copy-start.4 = (f32[512]{0:T(512)S(1)}, f32[512]{0:T(512)}, u32[]{:S(2)}) copy-start(f32[512]{0:T(512)} %param.10) | copy-start | bytes 6148
  13.6 11.0 %copy-start.5 = (f32[512]{0:T(512)S(1)}, f32[512]{0:T(512)}, u32[]{:S(2)}) copy-start(f32[512]{0:T(512)} %param.11) | copy-start | bytes 6148
  38.3 1.7 copy-start.1
  41.1 134.7 %reduce-scatter.5.cloned.1.call-start = ((), (), s32[]{:S(2)}) async-start(), calls=%async_computation.2 | async-start | bytes 4456448 | tf_op jit(solution)/shard_map/reduce_scatter | solution.py:43
  45.7 1.2 copy-start.2
  47.0 10.3 %copy-start.3 = (bf16[512,512]{1,0:T(8,128)(2,1)S(1)}, bf16[512,512]{1,0:T(8,128)(2,1)}, u32[]{:S(2)}) copy-start(bf16[512,512]{1,0:T(8,128)(2,1)} %param.8) | copy-start | bytes 1572868
  47.0 3.3 %collective-permute-start.1 = (f32[30,512]{1,0:T(8,128)S(1)}, f32[30,512]{1,0:T(8,128)S(1)}, u32[]{:S(2)}, u32[]{:S(2)}) collective-permute-start(f32[30,512]{1,0:T(8,128)S(1)} %slice.488), channel_id=1, source_target_pairs={{2,0},{4,2},{6,4},{8,6},{10,8},{12,10},{14,12},{16,14},{18,16},{20... | collective-permute-start | bytes 184328 | tf_op jit(solution)/shard_map/ppermute | solution.py:13
Sparse Core Ops, SparseCore 0:
  41.2 58.8 reduce-scatter.6
  103.9 71.7 reduce-scatter.4
